TPU v7x, 32 devices: a whole 2x2x4 slice. The times are simulated.
32 devices in a mesh: sp: 8 (over z, x), tp: 4 (over y, core).
Axes of the slice: x: 2, y: 2, z: 4, core: 2. Of those that a mesh axis runs over, the one named last changes fastest.
Arguments:
- resid: bfloat16 [6144, 2048], P(('sp', 'tp')), may hold values from -6 to 6
- queries: bfloat16 [6144, 1024], P('sp', 'tp'), may hold values from -160 to 160
- keys: bfloat16 [6144, 1024], P('sp', 'tp'), may hold values from -6 to 6
- values: bfloat16 [6144, 1024], P('sp', 'tp'), may hold values from -6 to 6
- cum_gate: float32 [6144, 16], P('sp', 'tp'), may hold values from -694 to 0, as said below
- out_weight: bfloat16 [1024, 2048], P('tp'), may hold values from -0.375 to 0.375
- norm_gain: float32 [2048], replicated, may hold values from 0.1 to 1.9
- gate_weight: bfloat16 [2048, 5504], P('sp', 'tp'), may hold values from -0.125 to 0.125
- up_weight: bfloat16 [2048, 5504], P('sp', 'tp'), may hold values from -0.125 to 0.125
- down_weight: bfloat16 [5504, 2048], P('tp', 'sp'), may hold values from -0.078125 to 0.078125
Outputs:
- layer_out: bfloat16 [6144, 2048], P(('sp', 'tp'))
Inputs may be any that keep to these rules, and one draw needn't show every extreme that they name: `cum_gate`: each column is non-increasing along positions and starts at or below zero.
All inputs are finite; a program needn't handle non-finite values.
Results may differ from a plain program's by a relative error of at most 0.01.
Values may be sent and summed in bfloat16 or wider, within the bound.
No kernel may reach another device: no remote copies, remote signals or barrier semaphores. Data moves between devices by JAX's collectives and lax.ppermute only.
A program may use at most 256 MiB of HBM per device.

v0:
```python
import jax
import jax.numpy as jnp
from jax import lax
from jax.sharding import PartitionSpec as P

HEAD_DIM = 64


def rms_norm(mixed, norm_gain):
    scaled = mixed * lax.rsqrt(jnp.mean(mixed * mixed, axis=-1, keepdims=True) + 1e-06) * norm_gain
    return scaled.astype(jnp.bfloat16)


def rounded(term):
    return term.astype(jnp.bfloat16).astype(jnp.float32)


def local(
    resid,
    queries,
    keys,
    values,
    cum_gate,
    out_weight,
    norm_gain,
    gate_weight,
    up_weight,
    down_weight,
):
    rows = queries.shape[0]
    heads_here = cum_gate.shape[1]
    scale = HEAD_DIM ** (-0.5)
    proj_weight = lax.all_gather(out_weight, "tp", axis=0, tiled=True)
    first = lax.axis_index("sp") * rows
    gates_all = lax.all_gather(cum_gate, "sp", axis=0, tiled=True)
    query_heads = queries.reshape(rows, heads_here, HEAD_DIM)
    query_pos = first + jnp.arange(rows, dtype=jnp.int32)
    query_gate = cum_gate.T
    best = jnp.full((heads_here, rows), -1e30, jnp.float32)
    key_piece = lax.all_gather(keys, "sp", axis=0, tiled=True)
    value_piece = lax.all_gather(values, "sp", axis=0, tiled=True)
    count = key_piece.shape[0]
    key_heads = key_piece.reshape(count, heads_here, HEAD_DIM)
    value_heads = value_piece.reshape(count, heads_here, HEAD_DIM)
    key_gate = gates_all.T
    score = (
        jnp.einsum("qhd,khd->hqk", query_heads, key_heads, preferred_element_type=jnp.float32)
        * scale
    )
    score = score + query_gate[:, :, None] - key_gate[:, None, :]
    key_pos = jnp.arange(count, dtype=jnp.int32)
    score = jnp.where(key_pos[None, None, :] <= query_pos[None, :, None], score, -jnp.inf)
    new_best = jnp.maximum(best, jnp.max(score, axis=-1))
    weight = jnp.exp(score - new_best[:, :, None])
    total = jnp.sum(weight, axis=-1)
    numer = jnp.einsum(
        "hqk,khd->hqd", weight.astype(jnp.bfloat16), value_heads, preferred_element_type=jnp.float32
    )
    best, total, numer = (new_best, total, numer)
    attn = (
        (numer / total[:, :, None])
        .transpose(1, 0, 2)
        .reshape(rows, heads_here * HEAD_DIM)
        .astype(jnp.bfloat16)
    )
    groups = lax.axis_size("tp")
    share = rows // groups
    own_rows = lax.all_to_all(attn, "tp", split_axis=0, concat_axis=1, tiled=True)
    group_width = attn.shape[1]
    row_groups = own_rows.reshape(share, groups, group_width)
    weight_groups = proj_weight.reshape(groups, group_width, proj_weight.shape[1])
    terms = jnp.einsum(
        "rgc,gcd->grd", row_groups, weight_groups, preferred_element_type=jnp.float32
    )
    proj = jnp.sum(rounded(terms), axis=0)
    mixed = resid.astype(jnp.float32) + proj
    normed_all = lax.all_gather(rms_norm(mixed, norm_gain), "tp", axis=0, tiled=True)
    gate_sum = jnp.dot(
        normed_all,
        lax.all_gather(gate_weight, "sp", axis=0, tiled=True),
        preferred_element_type=jnp.float32,
    )
    up_sum = jnp.dot(
        normed_all,
        lax.all_gather(up_weight, "sp", axis=0, tiled=True),
        preferred_element_type=jnp.float32,
    )
    hidden = (jax.nn.silu(gate_sum) * up_sum).astype(jnp.bfloat16)
    ffn_part = jnp.dot(
        hidden,
        lax.all_gather(down_weight, "sp", axis=1, tiled=True),
        preferred_element_type=jnp.float32,
    )
    ffn = lax.psum_scatter(
        rounded(ffn_part).astype(jnp.bfloat16), "tp", scatter_dimension=0, tiled=True
    ).astype(jnp.float32)
    return (mixed + 0.5 * ffn).astype(jnp.bfloat16)


def solution(mesh):
    in_specs = (
        P(("sp", "tp"), None),
        P("sp", "tp"),
        P("sp", "tp"),
        P("sp", "tp"),
        P("sp", "tp"),
        P("tp", None),
        P(),
        P("sp", "tp"),
        P("sp", "tp"),
        P("tp", "sp"),
    )
    out_specs = P(("sp", "tp"), None)
    return jax.shard_map(local, mesh=mesh, in_specs=in_specs, out_specs=out_specs, check_vma=False)
```

profile of v0, /device:TPU:0, one launch (start us, length us, event | category | flops | bytes accessed | tf_op | source)
XLA Modules:
  0.0 547.3 jit_solution(295551948475313620)
XLA Ops:
  6.5 0.7 all-gather.8.cloned.1.call-update
  7.3 0.7 all-gather.10.cloned.1.call-update
  8.1 0.7 all-gather.12.cloned.1.call-update
  8.8 0.5 all-gather.16.cloned.1.call-update
  9.4 5.7 %iota_compare_fusion = pred[768,6144]{1,0:T(8,128)(4,1)} fusion(s32[768]{0:T(1024)S(1)} %iota_add_fusion), kind=kLoop, calls=%fused_computation.7 | loop fusion | flops 4718592 | bytes 4721664 | tf_op jit(solution)/shard_map/le | solution.py:52
  15.1 32.9 %all_gather.25 = f32[6144,4]{0,1:T(4,128)S(1)} all-gather(f32[768,4]{0,1:T(4,128)S(1)} %copy-done.2), channel_id=1, replica_groups=mesh['sp'=8,'tp'=4] {'sp'}, dimensions={0}, use_global_device_ids=true | all-gather | bytes 110592 | tf_op jit(solution)/shard_map/all_gather | solution.py:35
  48.0 0.9 copy.15
  48.9 23.7 %all-gather.8.cloned.1.call-done = bf16[6144,256]{1,0:T(8,128)(2,1)} async-done(((bf16[768,256]{1,0:T(8,128)(2,1)}), bf16[6144,256]{1,0:T(8,128)(2,1)}) %all-gather.8.cloned.1.call-update) | async-done | bytes 3145744 | tf_op jit(solution)/shard_map/all_gather | solution.py:40
  72.6 3.5 copy.16
  76.2 31.1 %fusion.2 = (f32[4,768]{1,0:T(4,128)S(1)}, f32[4,768,6144]{2,1,0:T(8,128)}) fusion(f32[4,6144]{1,0:T(4,128)S(1)} %bitcast.30, f32[4,768]{1,0:T(4,128)S(1)} %bitcast.34, pred[768,6144]{1,0:T(8,128)(4,1)} %iota_compare_fusion, bf16[768,4,64]{0,2,1:T(8,128)(2,1)} %bitcast.33, bf16[6144,4,64]{0,2,1:T(8,128)(2,1)S(1)} %bitcast.29), kind=kOutput, calls=%fused_computation.4 | convolution fusion | flops 2510287872 | bytes 83877888 | tf_op jit(solution)/shard_map/qhd,khd->hqk/dot_general | solution.py:47
  107.3 26.4 %all-gather.10.cloned.1.call-done = bf16[6144,256]{1,0:T(8,128)(2,1)} async-done(((bf16[768,256]{1,0:T(8,128)(2,1)}), bf16[6144,256]{1,0:T(8,128)(2,1)}) %all-gather.10.cloned.1.call-update) | async-done | bytes 3145744 | tf_op jit(solution)/shard_map/all_gather | solution.py:41
  133.7 3.2 copy.17
  136.8 30.4 %fusion = f32[4,768]{1,0:T(4,128)S(1)} fusion(f32[4,768,6144]{2,1,0:T(8,128)} %get-tuple-element.6, f32[4,768]{1,0:T(4,128)S(1)} %broadcast_maximum_fusion, f32[4,6144]{1,0:T(4,128)S(1)} %bitcast.31, f32[4,768]{1,0:T(4,128)S(1)} %bitcast.35, pred[768,6144]{1,0:T(8,128)(4,1)} %iota_compare_fusion), kind=kLoop, calls=%fused_computation.2 | loop fusion | flops 113243136 | bytes 80351232 | tf_op jit(solution)/shard_map/reduce_sum | solution.py:55
  167.2 31.7 %fusion.12 = bf16[768,4,64]{0,2,1:T(8,128)(2,1)} fusion(bf16[6144,4,64]{0,2,1:T(8,128)(2,1)S(1)} %bitcast.28, f32[4,768,6144]{2,1,0:T(8,128)} %get-tuple-element.6, f32[4,768]{1,0:T(4,128)S(1)} %broadcast_maximum_fusion, f32[4,6144]{1,0:T(4,128)S(1)} %bitcast.32, f32[4,768]{1,0:T(4,128)S(1)} %bitcast.36, pred[768,6144]{1,0:T(8,128)(4,1)} %iota_compare_fusion, ...), kind=kOutput, calls=%fused_computation.18 | convolution fusion | flops 2529558528 | bytes 83890176 | tf_op jit(solution)/shard_map/hqk,khd->hqd/dot_general | solution.py:56
  198.9 1.5 convert_element_type.39
  200.4 0.3 copy.18
  200.7 9.9 %all_to_all.13 = bf16[4,192,256]{2,1,0:T(8,128)(2,1)S(1)} all-to-all(bf16[4,192,256]{2,1,0:T(8,128)(2,1)S(1)} %copy.18), channel_id=1, replica_groups=mesh['sp'=8,'tp'=4] {'tp'}, dimensions={0} | all-to-all | bytes 786432 | tf_op jit(solution)/shard_map/all_to_all | solution.py:68
  210.7 3.5 convert_reduce_fusion
  214.2 0.3 multiply_reduce_fusion
  214.5 1.1 multiply_convert_fusion.1
  215.6 0.0 all-gather.18.cloned.1.call-start
  215.7 0.5 all-gather.18.cloned.1.call-update
  216.3 0.7 all-gather.20.cloned.1.call-update
  217.0 8.7 %reduce-scatter.2.cloned.1.call-start = ((), (), s32[]{:S(2)}) async-start(), calls=%async_computation.9 | async-start | bytes 3932160 | tf_op jit(solution)/shard_map/reduce_scatter | solution.py:94
  225.7 36.2 %all-gather.16.cloned.1.call-done = bf16[2048,1376]{0,1:T(8,128)(2,1)} async-done(((bf16[256,1376]{0,1:T(8,128)(2,1)}), bf16[2048,1376]{0,1:T(8,128)(2,1)}) %all-gather.16.cloned.1.call-update) | async-done | bytes 5636112 | tf_op jit(solution)/shard_map/all_gather | solution.py:80
  261.9 28.1 %all-gather.14.cloned.1.call-done = bf16[768,2048]{1,0:T(8,128)(2,1)} async-done(((bf16[192,2048]{1,0:T(8,128)(2,1)}), bf16[768,2048]{1,0:T(8,128)(2,1)}) %all-gather.14.cloned.1.call-update) | async-done | bytes 3145744 | tf_op jit(solution)/shard_map/all_gather | solution.py:77
  290.0 10.2 %fusion.19 = f32[768,1376]{0,1:T(8,128)} fusion(bf16[768,2048]{1,0:T(8,128)(2,1)} %all-gather.14.cloned.1.call-done, bf16[2048,1376]{0,1:T(8,128)(2,1)} %all-gather.16.cloned.1.call-done), kind=kOutput, calls=%fused_computation.26 | convolution fusion | flops 4328521728 | bytes 13008896 | tf_op jit(solution)/shard_map/dot_general | solution.py:78
  300.2 83.3 %all-gather.18.cloned.1.call-done = bf16[2048,1376]{0,1:T(8,128)(2,1)} async-done(((bf16[256,1376]{0,1:T(8,128)(2,1)}), bf16[2048,1376]{0,1:T(8,128)(2,1)}) %all-gather.18.cloned.1.call-update) | async-done | bytes 5636112 | tf_op jit(solution)/shard_map/all_gather | solution.py:85
  383.5 91.8 %all-gather.20.cloned.1.call-done = bf16[1376,2048]{1,0:T(8,128)(2,1)} async-done(((bf16[1376,256]{1,0:T(8,128)(2,1)}), bf16[1376,2048]{1,0:T(8,128)(2,1)}) %all-gather.20.cloned.1.call-update) | async-done | bytes 5636112 | tf_op jit(solution)/shard_map/all_gather | solution.py:91
  475.3 26.4 %convolution_convert_fusion.1 = bf16[768,2048]{1,0:T(8,128)(2,1)} fusion(bf16[1376,2048]{1,0:T(8,128)(2,1)} %all-gather.20.cloned.1.call-done, f32[768,1376]{0,1:T(8,128)} %fusion.19, bf16[768,2048]{1,0:T(8,128)(2,1)} %all-gather.14.cloned.1.call-done, bf16[2048,1376]{0,1:T(8,128)(2,1)} %all-gather.18.cloned.1.call-done), kind=kOutput, calls=%fused_computation.11 | convolution fusion | flops 8664956928 | bytes 21790720 | tf_op jit(solution)/shard_map/dot_general | solution.py:89
  501.7 36.2 %reduce-scatter.2.cloned.1.call-done = bf16[192,2048]{1,0:T(8,128)(2,1)} async-done(((bf16[768,2048]{1,0:T(8,128)(2,1)}), bf16[192,2048]{1,0:T(8,128)(2,1)}) %reduce-scatter.2.cloned.1.call-update) | async-done | bytes 786448 | tf_op jit(solution)/shard_map/reduce_scatter | solution.py:94
  537.9 2.3 add_convert_fusion
  (20 shorter events, 0.3 us)
Async XLA Ops:
  6.5 8.6 %copy-start.2 = (f32[768,4]{0,1:T(4,128)S(1)}, f32[768,4]{0,1:T(4,128)}, u32[]{:S(2)}) copy-start(f32[768,4]{0,1:T(4,128)} %param.14) | copy-start | bytes 36868
  6.5 41.4 %copy-start.1 = (bf16[768,256]{1,0:T(8,128)(2,1)S(1)}, bf16[768,256]{1,0:T(8,128)(2,1)}, u32[]{:S(2)}) copy-start(bf16[768,256]{1,0:T(8,128)(2,1)} %param.11) | copy-start | bytes 1179652
  6.5 66.1 %all-gather.8.cloned.1.call-start = ((), (), s32[]{:S(2)}) async-start(), calls=%async_computation.2 | async-start | bytes 3538944 | tf_op jit(solution)/shard_map/all_gather | solution.py:40
  7.3 126.4 %all-gather.10.cloned.1.call-start = ((), (), s32[]{:S(2)}) async-start(), calls=%async_computation.3 | async-start | bytes 3538944 | tf_op jit(solution)/shard_map/all_gather | solution.py:41
  8.0 202.7 %all-gather.12.cloned.1.call-start = ((), (), s32[]{:S(2)}) async-start(), calls=%async_computation.4 | async-start | bytes 5242880 | tf_op jit(solution)/shard_map/all_gather | solution.py:33
  8.7 253.1 %all-gather.16.cloned.1.call-start = ((), (), s32[]{:S(2)}) async-start(), calls=%async_computation.6 | async-start | bytes 6340608 | tf_op jit(solution)/shard_map/all_gather | solution.py:80
  9.3 280.7 %all-gather.14.cloned.1.call-start = ((), (), s32[]{:S(2)}) async-start(), calls=%async_computation.5 | async-start | bytes 3932160 | tf_op jit(solution)/shard_map/all_gather | solution.py:77
  200.7 13.4 %copy-start = (bf16[192,2048]{1,0:T(8,128)(2,1)S(1)}, bf16[192,2048]{1,0:T(8,128)(2,1)}, u32[]{:S(2)}) copy-start(bf16[192,2048]{1,0:T(8,128)(2,1)} %param.10) | copy-start | bytes 2359300
  210.7 3.8 copy-start.3
  215.6 167.8 %all-gather.18.cloned.1.call-start = ((), (), s32[]{:S(2)}) async-start(), calls=%async_computation.7 | async-start | bytes 6340608 | tf_op jit(solution)/shard_map/all_gather | solution.py:85
  216.2 259.1 %all-gather.20.cloned.1.call-start = ((), (), s32[]{:S(2)}) async-start(), calls=%async_computation.8 | async-start | bytes 6340608 | tf_op jit(solution)/shard_map/all_gather | solution.py:91
  217.0 321.0 %reduce-scatter.2.cloned.1.call-start = ((), (), s32[]{:S(2)}) async-start(), calls=%async_computation.9 | async-start | bytes 3932160 | tf_op jit(solution)/shard_map/reduce_scatter | solution.py:94
Sparse Core Ops, SparseCore 0:
  9.5 63.0 all-gather.7
  74.8 58.8 all-gather.9
  135.2 33.1 all-gather.11
  170.3 91.5 all-gather.15
  263.3 26.6 all-gather.13
  291.9 91.5 all-gather.17
  385.5 89.7 all-gather.19
  501.8 36.0 reduce-scatter.1
where the time goes:
time: 551 us; the launch traced here: 547 us
  waiting for transfers between devices  330 us (60%)
  matrix products  103 us (19%)
  blocking collectives  42.8 us (8%)
  other arithmetic  39.9 us (7%)
  between operations  13.8 us (3%)
  local copies, waits for them, and re-layouts  9.49 us (2%)
  starting transfers between devices  8.97 us (2%)
    all_gather x1, waiting for transfers between devices, local(): lax.all_gather(down_weight, 'sp', axis=1, tiled=True)  91.8 us
    all_gather x1, waiting for transfers between devices, local(): lax.all_gather(up_weight, 'sp', axis=0, tiled=True)  83.3 us
    reduce_scatter x1, waiting for transfers between devices, local(): lax.psum_scatter(rounded(ffn_part).astype(jnp.bfloat16), 'tp', scatter_di...  36.2 us
    all_gather x1, waiting for transfers between devices, local(): lax.all_gather(gate_weight, 'sp', axis=0, tiled=True)  36.2 us
    all_gather x1, blocking collectives, local(): gates_all = lax.all_gather(cum_gate, 'sp', axis=0, tiled=True)  32.9 us
    dot_general x1, matrix products, local(): jnp.einsum('hqk,khd->hqd', weight.astype(jnp.bfloat16), value_heads, pref...  31.7 us
    dot_general x1, matrix products, local(): jnp.einsum('qhd,khd->hqk', query_heads, key_heads, preferred_element_type...  31.1 us
    reduce_sum x1, other arithmetic, local(): total = jnp.sum(weight, axis=-1)  30.4 us
  transfers between devices with their start and end apart: 8, of which 7 were waited for; matrix products, arithmetic and copies ran while one was open for 23% of the time, Pallas kernels for 0%

commit v1 on v0

--- a/solution.py
+++ b/solution.py
@@ -2,6 +2,7 @@
 import jax.numpy as jnp
 from jax import lax
 from jax.sharding import PartitionSpec as P
+from jax.lax import all_gather
 
 HEAD_DIM = 64
 
@@ -32,12 +33,19 @@
     scale = HEAD_DIM ** (-0.5)
     proj_weight = lax.all_gather(out_weight, "tp", axis=0, tiled=True)
     first = lax.axis_index("sp") * rows
-    gates_all = lax.all_gather(cum_gate, "sp", axis=0, tiled=True)
     query_heads = queries.reshape(rows, heads_here, HEAD_DIM)
     query_pos = first + jnp.arange(rows, dtype=jnp.int32)
     query_gate = cum_gate.T
     best = jnp.full((heads_here, rows), -1e30, jnp.float32)
-    key_piece = lax.all_gather(keys, "sp", axis=0, tiled=True)
+
+    def guide_cubes(u_in, original):
+        return jnp.split(
+            all_gather(jnp.concatenate([u_in, original], axis=1), "sp", axis=0, tiled=True),
+            [u_in.shape[1]],
+            axis=1,
+        )
+
+    gates_all, key_piece = guide_cubes(cum_gate, keys)
     value_piece = lax.all_gather(values, "sp", axis=0, tiled=True)
     count = key_piece.shape[0]
     key_heads = key_piece.reshape(count, heads_here, HEAD_DIM)

time: 551 us -> 628 us (1.14)
  waiting for transfers between devices: 330 us -> 441 us
  blocking collectives: 42.8 us -> 0 us
  local copies, waits for them, and re-layouts: 9.49 us -> 21.3 us
    all_gather x1, waiting for transfers between devices: 23.7 us -> 133 us  [guide_cubes(): all_gather(jnp.concatenate([u_in, original], axis=1), 'sp', axis=0, tiled...]
    all_gather x1 -> x0, blocking collectives: 32.9 us -> none  [local(): gates_all = lax.all_gather(cum_gate, 'sp', axis=0, tiled=True)]
    all_gather x1, waiting for transfers between devices: 36.2 us -> 4.82 us  [local(): lax.all_gather(gate_weight, 'sp', axis=0, tiled=True)]
    all_gather x1, waiting for transfers between devices: 26.4 us -> 53 us  [local(): value_piece = lax.all_gather(values, 'sp', axis=0, tiled=True)]
    all_to_all x1 -> x0, blocking collectives: 9.94 us -> none  [local(): lax.all_to_all(attn, 'tp', split_axis=0, concat_axis=1, tiled=True)]
    reduce_scatter x1, starting transfers between devices: 8.74 us -> 0.21 us  [local(): lax.psum_scatter(rounded(ffn_part).astype(jnp.bfloat16), 'tp', scatter_di...]
    split x0 -> x2, local copies, waits for them, and re-layouts: none -> 8.44 us  [guide_cubes(): jnp.split(all_gather(jnp.concatenate([u_in, original], axis=1), 'sp', axi...]
    all_to_all x0 -> x1, waiting for transfers between devices: none -> 7.3 us  [local(): lax.all_to_all(attn, 'tp', split_axis=0, concat_axis=1, tiled=True)]
  transfers between devices with their start and end apart: 8 -> 9, of which waited for: 7 -> 8; matrix products, arithmetic and copies ran while one was open for 23% -> 22% of each run, Pallas kernels for 0% -> 0%
where the time goes in v1:
time: 628 us; the launch traced here: 624 us
  waiting for transfers between devices  441 us (70%)
  matrix products  102 us (16%)
  other arithmetic  41.4 us (7%)
  local copies, waits for them, and re-layouts  21.3 us (3%)
  between operations  13.8 us (2%)
    all_gather x1, waiting for transfers between devices, guide_cubes(): all_gather(jnp.concatenate([u_in, original], axis=1), 'sp', axis=0, tiled...  133 us
    all_gather x1, waiting for transfers between devices, local(): lax.all_gather(down_weight, 'sp', axis=1, tiled=True)  91.8 us
    all_gather x1, waiting for transfers between devices, local(): lax.all_gather(up_weight, 'sp', axis=0, tiled=True)  83.3 us
    all_gather x1, waiting for transfers between devices, local(): value_piece = lax.all_gather(values, 'sp', axis=0, tiled=True)  53 us
    reduce_scatter x1, waiting for transfers between devices, local(): lax.psum_scatter(rounded(ffn_part).astype(jnp.bfloat16), 'tp', scatter_di...  36.2 us
    dot_general x1, matrix products, local(): jnp.einsum('qhd,khd->hqk', query_heads, key_heads, preferred_element_type...  32.5 us
    dot_general x1, matrix products, local(): jnp.einsum('hqk,khd->hqd', weight.astype(jnp.bfloat16), value_heads, pref...  29.9 us
    reduce_sum x1, other arithmetic, local(): total = jnp.sum(weight, axis=-1)  28.8 us
  transfers between devices with their start and end apart: 9, of which 8 were waited for; matrix products, arithmetic and copies ran while one was open for 22% of the time, Pallas kernels for 0%

profile of v1, /device:TPU:0, one launch (start us, length us, event | category | flops | bytes accessed | tf_op | source)
XLA Modules:
  0.0 623.6 jit_solution(1500317411411300822)
XLA Ops:
  6.5 0.7 all-gather.10.cloned.1.call-update
  7.3 1.0 convert_element_type.40
  8.4 0.9 copy.18
  9.3 1.5 pad_maximum_fusion
  10.8 0.7 all-gather.12.cloned.1.call-update
  12.1 6.3 %iota_compare_fusion = pred[768,6144]{0,1:T(8,128)(4,1)} fusion(s32[768]{0:T(1024)S(1)} %iota_add_fusion), kind=kLoop, calls=%fused_computation.7 | loop fusion | flops 4718592 | bytes 4721664 | tf_op jit(solution)/shard_map/le | solution.py:60
  18.4 0.9 copy.20
  19.3 53.0 %all-gather.10.cloned.1.call-done = bf16[6144,256]{1,0:T(8,128)(2,1)} async-done(((bf16[768,256]{1,0:T(8,128)(2,1)}), bf16[6144,256]{1,0:T(8,128)(2,1)}) %all-gather.10.cloned.1.call-update) | async-done | bytes 3145744 | tf_op jit(solution)/shard_map/all_gather | solution.py:49
  72.3 5.2 copy.22
  77.4 133.0 %all-gather.8.cloned.1.call-done = f32[6144,260]{1,0:T(8,128)} async-done(((f32[768,260]{1,0:T(8,128)}), f32[6144,260]{1,0:T(8,128)}) %all-gather.8.cloned.1.call-update) | async-done | bytes 6389776 | tf_op jit(solution)/shard_map/all_gather | solution.py:43
  210.4 2.1 slice_bitcast_fusion
  212.5 1.2 copy.21
  213.7 5.3 split.8
  219.0 3.1 copy.19
  222.2 32.5 %fusion.2 = (f32[4,768]{1,0:T(4,128)S(1)}, f32[4,6144,768]{2,1,0:T(8,128)}) fusion(f32[4,6144]{1,0:T(4,128)S(1)} %copy.21, f32[4,768]{1,0:T(4,128)S(1)} %bitcast.41, pred[768,6144]{0,1:T(8,128)(4,1)} %iota_compare_fusion, bf16[6144,4,64]{0,2,1:T(8,128)(2,1)} %bitcast.39, bf16[768,4,64]{0,2,1:T(8,128)(2,1)} %bitcast.40), kind=kOutput, calls=%fused_computation.4 | convolution fusion | flops 2510287872 | bytes 83877888 | tf_op jit(solution)/shard_map/qhd,khd->hqk/dot_general | solution.py:55
  254.7 28.8 %fusion = f32[4,768]{1,0:T(4,128)S(1)} fusion(f32[4,6144,768]{2,1,0:T(8,128)} %get-tuple-element.6, f32[4,768]{1,0:T(4,128)S(1)} %broadcast_maximum_fusion, f32[4,6144]{1,0:T(4,128)S(1)} %copy.21, f32[4,768]{1,0:T(4,128)S(1)} %bitcast.42, pred[768,6144]{0,1:T(8,128)(4,1)} %iota_compare_fusion), kind=kLoop, calls=%fused_computation.2 | loop fusion | flops 113243136 | bytes 80351232 | tf_op jit(solution)/shard_map/reduce_sum | solution.py:63
  283.5 29.9 %divide_convert_fusion = bf16[768,4,64]{0,2,1:T(8,128)(2,1)} fusion(f32[768,4]{0,1:T(4,128)S(1)} %bitcast.44, bf16[6144,4,64]{0,2,1:T(8,128)(2,1)S(1)} %bitcast.38, f32[4,6144,768]{2,1,0:T(8,128)} %get-tuple-element.6, f32[4,768]{1,0:T(4,128)S(1)} %broadcast_maximum_fusion, f32[4,6144]{1,0:T(4,128)S(1)} %copy.21, f32[4,768]{1,0:T(4,128)S(1)} %bitcast.43, ...), kind=kOutput, calls=%fused_computation.19 | convolution fusion | flops 2529558528 | bytes 83890176 | tf_op jit(solution)/shard_map/hqk,khd->hqd/dot_general | solution.py:64
  313.4 1.5 convert_element_type.43
  314.9 1.1 copy.24
  316.0 3.6 all-to-all-start
  319.7 7.3 %all-to-all-done = bf16[4,192,256]{2,1,0:T(8,128)(2,1)S(1)} async-done(((bf16[4,192,256]{2,1,0:T(8,128)(2,1)}), bf16[4,192,256]{2,1,0:T(8,128)(2,1)S(1)}, u32[]{:S(2)}, u32[]{:S(2)}) %all-to-all-start) | async-done | bytes 393248 | tf_op jit(solution)/shard_map/all_to_all | solution.py:76
  327.0 3.3 convert_reduce_fusion
  330.6 1.1 multiply_convert_fusion.1
  332.4 0.7 all-gather.20.cloned.1.call-update
  333.3 4.8 all-gather.16.cloned.1.call-done
  338.1 28.1 %all-gather.14.cloned.1.call-done = bf16[768,2048]{1,0:T(8,128)(2,1)} async-done(((bf16[192,2048]{1,0:T(8,128)(2,1)}), bf16[768,2048]{1,0:T(8,128)(2,1)}) %all-gather.14.cloned.1.call-update) | async-done | bytes 3145744 | tf_op jit(solution)/shard_map/all_gather | solution.py:85
  366.3 10.2 %fusion.13 = f32[768,1376]{0,1:T(8,128)} fusion(bf16[768,2048]{1,0:T(8,128)(2,1)} %all-gather.14.cloned.1.call-done, bf16[2048,1376]{0,1:T(8,128)(2,1)} %all-gather.16.cloned.1.call-done), kind=kOutput, calls=%fused_computation.27 | convolution fusion | flops 4328521728 | bytes 13008896 | tf_op jit(solution)/shard_map/dot_general | solution.py:86
  376.4 83.3 %all-gather.18.cloned.1.call-done = bf16[2048,1376]{0,1:T(8,128)(2,1)} async-done(((bf16[256,1376]{0,1:T(8,128)(2,1)}), bf16[2048,1376]{0,1:T(8,128)(2,1)}) %all-gather.18.cloned.1.call-update) | async-done | bytes 5636112 | tf_op jit(solution)/shard_map/all_gather | solution.py:93
  459.7 91.8 %all-gather.20.cloned.1.call-done = bf16[1376,2048]{1,0:T(8,128)(2,1)} async-done(((bf16[1376,256]{1,0:T(8,128)(2,1)}), bf16[1376,2048]{1,0:T(8,128)(2,1)}) %all-gather.20.cloned.1.call-update) | async-done | bytes 5636112 | tf_op jit(solution)/shard_map/all_gather | solution.py:99
  551.5 26.4 %convolution_convert_fusion.1 = bf16[768,2048]{1,0:T(8,128)(2,1)} fusion(bf16[1376,2048]{1,0:T(8,128)(2,1)} %all-gather.20.cloned.1.call-done, f32[768,1376]{0,1:T(8,128)} %fusion.13, bf16[768,2048]{1,0:T(8,128)(2,1)} %all-gather.14.cloned.1.call-done, bf16[2048,1376]{0,1:T(8,128)(2,1)} %all-gather.18.cloned.1.call-done), kind=kOutput, calls=%fused_computation.11 | convolution fusion | flops 8664956928 | bytes 21790720 | tf_op jit(solution)/shard_map/dot_general | solution.py:97
  578.0 36.2 %reduce-scatter.2.cloned.1.call-done = bf16[192,2048]{1,0:T(8,128)(2,1)} async-done(((bf16[768,2048]{1,0:T(8,128)(2,1)}), bf16[192,2048]{1,0:T(8,128)(2,1)}) %reduce-scatter.2.cloned.1.call-update) | async-done | bytes 786448 | tf_op jit(solution)/shard_map/reduce_scatter | solution.py:102
  614.2 2.3 add_convert_fusion
  (28 shorter events, 1.9 us)
Async XLA Ops:
  6.5 65.7 %all-gather.10.cloned.1.call-start = ((), (), s32[]{:S(2)}) async-start(), calls=%async_computation.3 | async-start | bytes 3538944 | tf_op jit(solution)/shard_map/all_gather | solution.py:49
  7.3 203.1 %all-gather.8.cloned.1.call-start = ((), (), s32[]{:S(2)}) async-start(), calls=%async_computation.2 | async-start | bytes 10616832 | tf_op jit(solution)/shard_map/all_gather | solution.py:43
  9.2 9.1 %copy-start.2 = (bf16[768,256]{1,0:T(8,128)(2,1)S(1)}, bf16[768,256]{1,0:T(8,128)(2,1)}, u32[]{:S(2)}) copy-start(bf16[768,256]{1,0:T(8,128)(2,1)} %param.11) | copy-start | bytes 1179652
  10.8 308.9 %all-gather.12.cloned.1.call-start = ((), (), s32[]{:S(2)}) async-start(), calls=%async_computation.4 | async-start | bytes 5242880 | tf_op jit(solution)/shard_map/all_gather | solution.py:34
  11.5 326.6 %all-gather.16.cloned.1.call-start = ((), (), s32[]{:S(2)}) async-start(), calls=%async_computation.6 | async-start | bytes 6340608 | tf_op jit(solution)/shard_map/all_gather | solution.py:88
  219.0 3.2 copy-start.3
  254.7 28.8 %copy-start.1 = (bf16[6144,256]{0,1:T(8,128)(2,1)S(1)}, bf16[6144,256]{0,1:T(8,128)(2,1)}, u32[]{:S(2)}) copy-start(bf16[6144,256]{0,1:T(8,128)(2,1)} %copy.22) | copy-start | bytes 9437188
  316.0 14.3 %copy-start = (bf16[192,2048]{1,0:T(8,128)(2,1)S(1)}, bf16[192,2048]{1,0:T(8,128)(2,1)}, u32[]{:S(2)}) copy-start(bf16[192,2048]{1,0:T(8,128)(2,1)} %param.10) | copy-start | bytes 2359300
  316.0 11.0 %all-to-all-start = ((bf16[4,192,256]{2,1,0:T(8,128)(2,1)}), bf16[4,192,256]{2,1,0:T(8,128)(2,1)S(1)}, u32[]{:S(2)}, u32[]{:S(2)}) async-start(bf16[4,192,256]{2,1,0:T(8,128)(2,1)} %copy.24), calls=%async_computation | async-start | bytes 786432 | tf_op jit(solution)/shard_map/all_to_all | solution.py:76
  319.6 46.6 %all-gather.14.cloned.1.call-start = ((), (), s32[]{:S(2)}) async-start(), calls=%async_computation.5 | async-start | bytes 3932160 | tf_op jit(solution)/shard_map/all_gather | solution.py:85
  327.0 3.6 copy-start.4
  331.8 128.0 %all-gather.18.cloned.1.call-start = ((), (), s32[]{:S(2)}) async-start(), calls=%async_computation.7 | async-start | bytes 6340608 | tf_op jit(solution)/shard_map/all_gather | solution.py:93
  332.3 219.2 %all-gather.20.cloned.1.call-start = ((), (), s32[]{:S(2)}) async-start(), calls=%async_computation.8 | async-start | bytes 6340608 | tf_op jit(solution)/shard_map/all_gather | solution.py:99
  333.1 281.1 %reduce-scatter.2.cloned.1.call-start = ((), (), s32[]{:S(2)}) async-start(), calls=%async_computation.9 | async-start | bytes 3932160 | tf_op jit(solution)/shard_map/reduce_scatter | solution.py:102
Sparse Core Ops, SparseCore 0:
  9.5 62.7 all-gather.9
  74.5 135.8 all-gather.7
  212.0 32.6 all-gather.11
  246.5 91.5 all-gather.15
  339.5 26.6 all-gather.13
  368.2 91.5 all-gather.17
  461.8 89.7 all-gather.19
  578.1 36.0 reduce-scatter.1
